TPU v7x, 32 devices: a whole 2x2x4 slice. The times are simulated.
32 devices in a mesh: ep: 8 (over z, x), tp: 4 (over y, core).
Axes of the slice: x: 2, y: 2, z: 4, core: 2. Of those that a mesh axis runs over, the one named last changes fastest.
Arguments:
- projected_queries: bfloat16 [2048, 2048], P('ep', 'tp'), may hold values from -245 to 245, as said below
- key_proj: bfloat16 [2048, 512], P('ep', 'tp'), may hold values from -6.2 to 6.2
- projected_values: bfloat16 [2048, 512], P('ep', 'tp'), may hold values from -24 to 24
- head_sink_logits: float32 [32], P('tp'), may hold values from 1 to 6
- out_weight: bfloat16 [2048, 4096], P('tp'), may hold values from -0.125 to 0.125
- expert_input: bfloat16 [1024, 4096], P('ep'), may hold values from -6 to 6
- norm_gain: float32 [4096], replicated, may hold values from 0.1 to 1.9
- routing: int32 [1024, 4], P('ep'), may hold values from 0 to 7, all different within a row; in each aligned block of 128 rows (0 to 127, 128 to 255, ...) at most 96 rows name the same one
- route_weight: float32 [1024, 4], P('ep'), may hold values from 0.1 to 1
- gate_weight: bfloat16 [8, 4096, 1024], P('ep', None, 'tp'), may hold values from -0.27929688 to 0.27929688
- up_weight: bfloat16 [8, 4096, 1024], P('ep', None, 'tp'), may hold values from -0.27929688 to 0.27929688
- down_weight: bfloat16 [8, 1024, 4096], P('ep', 'tp'), may hold values from -0.046875 to 0.046875
Outputs:
- mixer_output: bfloat16 [2048, 4096], P(('ep', 'tp'))
- expert_output: bfloat16 [1024, 4096], P('ep', 'tp')
Inputs may be any that keep to these rules, and one draw needn't show every extreme that they name: `projected_queries`: in the hidden draw some queries nearly equal a large multiple of a nearby key. `routing`: each row names 4 different experts; among the rows of one device (aligned blocks of 128 rows) no expert is named more than 96 times, a bound that some block reaches.
All inputs are finite; a program needn't handle non-finite values.
Results may differ from a plain program's by a relative error of at most 0.014.
Values may be sent and summed in bfloat16 or wider, within the bound.
A program may use at most 128 MiB of HBM per device.

v0:
```python
import jax
import jax.numpy as jnp
from jax import lax
from jax.sharding import PartitionSpec as P

D = 4096
HEAD_SIZE = 64
WINDOW_KEYS = 128
TOPK = 4


EPS = 1e-06
CLAMP = 7.0
SLOPE = 1.702


def passed_along(block, axis, distance):
    devices = range(lax.axis_size(axis))
    route = [(i - distance, i) for i in devices if i - distance in devices]
    return lax.ppermute(block, axis, route)


def shards(
    projected_queries,
    key_proj,
    projected_values,
    head_sink_logits,
    out_weight,
    expert_input,
    norm_gain,
    routing,
    route_weight,
    gate_weight,
    up_weight,
    down_weight,
):
    query_rows = projected_queries.shape[0]
    kv_heads = key_proj.shape[1] // HEAD_SIZE
    heads_per_group = projected_queries.shape[1] // HEAD_SIZE // kv_heads
    count_of_blocks = query_rows // WINDOW_KEYS
    prior_key, prior_value = passed_along(
        (key_proj[query_rows - WINDOW_KEYS :], projected_values[query_rows - WINDOW_KEYS :]),
        "ep",
        1,
    )
    key_all = jnp.concatenate([prior_key, key_proj], axis=0)
    value_all = jnp.concatenate([prior_value, projected_values], axis=0)
    window_keys = jnp.concatenate(
        [
            key_all[:-WINDOW_KEYS].reshape(count_of_blocks, WINDOW_KEYS, kv_heads, HEAD_SIZE),
            key_all[WINDOW_KEYS:].reshape(count_of_blocks, WINDOW_KEYS, kv_heads, HEAD_SIZE),
        ],
        axis=1,
    )
    window_values = jnp.concatenate(
        [
            value_all[:-WINDOW_KEYS].reshape(count_of_blocks, WINDOW_KEYS, kv_heads, HEAD_SIZE),
            value_all[WINDOW_KEYS:].reshape(count_of_blocks, WINDOW_KEYS, kv_heads, HEAD_SIZE),
        ],
        axis=1,
    )
    query_blocks = projected_queries.reshape(
        count_of_blocks, WINDOW_KEYS, kv_heads, heads_per_group, HEAD_SIZE
    )
    scores = jnp.einsum(
        "nqhgd,nshd->nhgqs", query_blocks, window_keys, preferred_element_type=jnp.float32
    ) * HEAD_SIZE ** (-0.5)
    offset = lax.axis_index("ep") * query_rows
    block_ids = jnp.arange(count_of_blocks)[:, None, None] * WINDOW_KEYS + offset
    query_pos = block_ids + jnp.arange(WINDOW_KEYS)[None, :, None]
    key_pos = block_ids - WINDOW_KEYS + jnp.arange(2 * WINDOW_KEYS)[None, None, :]
    permitted_mask = (key_pos <= query_pos) & (query_pos - key_pos < WINDOW_KEYS) & (key_pos >= 0)
    scores = jnp.where(permitted_mask[:, None, None, :, :], scores, -jnp.inf)
    sink_col = head_sink_logits.reshape(kv_heads, heads_per_group)[None, :, :, None, None]
    highest = jnp.maximum(jnp.max(scores, axis=-1, keepdims=True), sink_col)
    numerator = jnp.exp(scores - highest)
    denominator = jnp.sum(numerator, axis=-1, keepdims=True) + jnp.exp(sink_col - highest)
    weights = (numerator / denominator).astype(jnp.bfloat16)
    attended = jnp.einsum(
        "nhgqs,nshd->nqhgd", weights, window_values, preferred_element_type=jnp.float32
    )
    attended = attended.astype(jnp.bfloat16).reshape(
        query_rows, kv_heads * heads_per_group * HEAD_SIZE
    )
    mixer_output = lax.psum_scatter(
        jnp.dot(attended, out_weight, preferred_element_type=jnp.float32).astype(jnp.bfloat16),
        "tp",
        scatter_dimension=0,
        tiled=True,
    )
    token_rows = expert_input.shape[0]
    experts = lax.axis_size("ep")
    capacity = max(3 * token_rows * TOPK // (2 * experts), 2)
    col_share = D // lax.axis_size("tp")
    widened = expert_input.astype(jnp.float32)
    normed = (
        widened
        * lax.rsqrt(jnp.mean(widened * widened, axis=-1, keepdims=True) + EPS)
        * norm_gain[None, :]
    ).astype(jnp.bfloat16)
    flat_ids = routing.reshape(-1)
    onehot = (flat_ids[:, None] == jnp.arange(experts, dtype=jnp.int32)[None, :]).astype(jnp.int32)
    rank_in = jnp.cumsum(onehot, axis=0) - 1
    target = flat_ids * capacity + jnp.sum(rank_in * onehot, axis=1)
    tok_ids = jnp.arange(token_rows * TOPK) // TOPK
    slot_tok = jnp.full((experts * capacity,), token_rows, jnp.int32).at[target].set(tok_ids)
    gate_one = gate_weight[0]
    up_one = up_weight[0]
    own_cols = lax.dynamic_slice_in_dim(normed, lax.axis_index("tp") * col_share, col_share, 1)
    extended = jnp.concatenate([own_cols, jnp.zeros((1, col_share), jnp.bfloat16)], axis=0)
    outgoing = jnp.take(extended, slot_tok, axis=0).reshape(experts, capacity, col_share)
    arrived = lax.all_to_all(outgoing, "ep", split_axis=0, concat_axis=0, tiled=True).reshape(
        experts * capacity, col_share
    )
    portion = lax.all_gather(arrived, "tp", axis=1, tiled=True)
    gate_pre = jnp.dot(portion, gate_one, preferred_element_type=jnp.float32)
    up_pre = jnp.dot(portion, up_one, preferred_element_type=jnp.float32)
    gate_cut = jnp.minimum(gate_pre, CLAMP)
    activated = (
        (jnp.clip(up_pre, -CLAMP, CLAMP) + 1.0) * gate_cut * jax.nn.sigmoid(SLOPE * gate_cut)
    ).astype(jnp.bfloat16)
    partial_value = jnp.dot(activated, down_weight[0], preferred_element_type=jnp.float32)
    expert_result = lax.psum_scatter(
        partial_value.astype(jnp.bfloat16), "tp", scatter_dimension=1, tiled=True
    )
    returned = lax.all_to_all(
        expert_result.reshape(experts, capacity, col_share),
        "ep",
        split_axis=0,
        concat_axis=0,
        tiled=True,
    )
    picked = jnp.take(returned.reshape(experts * capacity, col_share), target, axis=0)
    picked = picked.astype(jnp.float32).reshape(token_rows, TOPK, col_share)
    expert_output = jnp.sum(picked * route_weight[:, :, None], axis=1).astype(jnp.bfloat16)
    return (mixer_output, expert_output)


def solution(mesh):
    placed = (
        P("ep", "tp"),
        P("ep", "tp"),
        P("ep", "tp"),
        P("tp"),
        P("tp", None),
        P("ep", None),
        P(),
        P("ep", None),
        P("ep", None),
        P("ep", None, "tp"),
        P("ep", None, "tp"),
        P("ep", "tp", None),
    )
    return jax.shard_map(
        shards,
        mesh=mesh,
        in_specs=placed,
        out_specs=(P(("ep", "tp"), None), P("ep", "tp")),
        check_vma=False,
    )
```

profile of v0, /device:TPU:0, one launch (start us, length us, event | category | flops | bytes accessed | tf_op | source)
XLA Modules:
  0.0 246.2 jit_solution(7340603953749888694)
XLA Ops:
  7.2 0.0 copy-start
  7.2 0.0 all-gather.2.cloned.1.call-start
  7.2 2.9 %convert_element_type.41 = f32[128,4096]{1,0:T(8,128)} convert(bf16[128,4096]{1,0:T(8,128)(2,1)} %param.17) | non-fusion elementwise | flops 524288 | bytes 3145728 | tf_op jit(solution)/shard_map/convert_element_type | solution.py:95
  10.2 0.3 multiply_reduce_fusion.1
  10.5 0.1 copy.46
  10.6 0.1 eq.26
  10.7 0.1 reshape.219
  10.8 1.1 reduce-window.6
  12.0 0.2 slice_reduce_fusion
  12.3 0.1 copy.50
  12.4 0.1 mul.95
  12.5 0.1 fusion.47
  12.6 2.4 scatter_custom_fusion
  15.1 0.1 broadcast_in_dim.55
  15.2 0.7 dynamic-slice
  15.9 1.1 fusion.33
  17.1 3.6 %gather_fusion = bf16[768,1024]{1,0:T(8,128)(2,1)} fusion(bf16[129,1024]{1,0:T(8,128)(2,1)S(1)} %concatenate.19, s32[1024]{0:T(1024)S(1)} %pad_clamp_fusion.1), kind=kCustom, calls=%fused_computation | custom fusion | bytes 3148800 | tf_op jit(solution)/shard_map/jit(_take)/gather | solution.py:111
  20.6 1.6 broadcast_select_fusion
  22.3 44.2 %all_to_all.10 = bf16[8,96,1024]{2,1,0:T(8,128)(2,1)} all-to-all(bf16[8,96,1024]{2,1,0:T(8,128)(2,1)S(1)} %broadcast_select_fusion), channel_id=1, replica_groups=mesh['ep'=8,'tp'=4] {'ep'}, dimensions={0} | all-to-all | bytes 3145728 | tf_op jit(solution)/shard_map/all_to_all | solution.py:112
  66.4 0.0 all-gather.2.cloned.1.call-update
  66.5 0.0 reduce-scatter.5.cloned.1.call-start
  66.5 45.5 %all-gather.2.cloned.1.call-done = bf16[768,4096]{1,0:T(8,128)(2,1)} async-done(((bf16[768,1024]{1,0:T(8,128)(2,1)}), bf16[768,4096]{1,0:T(8,128)(2,1)}) %all-gather.2.cloned.1.call-update) | async-done | bytes 6291472 | tf_op jit(solution)/shard_map/all_gather | solution.py:115
  112.0 5.2 %fusion.9 = f32[768,256]{1,0:T(8,128)S(1)} fusion(bf16[768,4096]{1,0:T(8,128)(2,1)} %all-gather.2.cloned.1.call-done, bf16[1,4096,256]{2,1,0:T(8,128)(2,1)} %param.21), kind=kOutput, calls=%fused_computation.18 | convolution fusion | flops 1610809344 | bytes 9175040 | tf_op jit(solution)/shard_map/dot_general | solution.py:116
  117.2 12.7 %convolution_convert_fusion = bf16[768,4096]{1,0:T(8,128)(2,1)} fusion(bf16[1,256,4096]{2,1,0:T(8,128)(2,1)S(1)} %copy-done, f32[768,256]{1,0:T(8,128)S(1)} %fusion.9, bf16[768,4096]{1,0:T(8,128)(2,1)} %all-gather.2.cloned.1.call-done, bf16[1,4096,256]{2,1,0:T(8,128)(2,1)} %param.22), kind=kOutput, calls=%fused_computation.3 | convolution fusion | flops 3226140672 | bytes 17563648 | tf_op jit(solution)/shard_map/dot_general | solution.py:122
  129.9 0.0 reduce-scatter.5.cloned.1.call-update
  130.0 0.0 reduce-scatter.3.cloned.1.call-start
  130.0 0.8 copy-done.3
  130.8 3.4 %collective-permute-start.1 = (bf16[128,128]{1,0:T(8,128)(2,1)S(1)}, bf16[128,128]{1,0:T(8,128)(2,1)S(1)}, u32[]{:S(2)}, u32[]{:S(2)}) collective-permute-start(bf16[128,128]{1,0:T(8,128)(2,1)S(1)} %slice.20), channel_id=1, source_target_pairs={{0,4},{4,8},{8,12},{12,16},{16,20},{20,24},{24,28},{1,5},{5,9},{9,... | collective-permute-start | bytes 98312 | tf_op jit(solution)/shard_map/ppermute | solution.py:20
  134.2 3.6 %collective-permute-start = (bf16[128,128]{1,0:T(8,128)(2,1)S(1)}, bf16[128,128]{1,0:T(8,128)(2,1)S(1)}, u32[]{:S(2)}, u32[]{:S(2)}) collective-permute-start(bf16[128,128]{1,0:T(8,128)(2,1)S(1)} %slice.18), channel_id=1, source_target_pairs={{0,4},{4,8},{8,12},{12,16},{16,20},{20,24},{24,28},{1,5},{5,9},{9,... | collective-permute-start | bytes 98312 | tf_op jit(solution)/shard_map/ppermute | solution.py:20
  137.7 0.1 broadcast_compare_fusion
  137.8 0.1 iota_add_fusion.1
  137.9 0.1 iota_add_fusion
  138.0 0.2 fusion.42
  138.2 0.1 reshape.254
  138.3 0.1 reshape.252
  138.4 0.3 reshape.255
  138.7 0.1 copy.41
  138.8 0.1 max.24
  138.9 0.1 copy.37
  139.0 0.1 reshape.253
  139.1 0.1 copy.40
  139.2 0.1 reshape.251
  139.4 0.1 copy.36
  139.5 0.5 fusion.60
  140.0 0.1 broadcast_maximum_fusion
  140.1 0.3 fusion.5
  140.4 0.1 exponential_add_fusion
  140.5 0.0 copy-start.2
  140.5 0.5 fusion.26
  141.0 0.3 copy.45
  141.2 1.7 copy-done.2
  143.0 2.7 %convolution_convert_fusion.1 = bf16[256,4096]{1,0:T(8,128)(2,1)} fusion(bf16[512,4096]{1,0:T(8,128)(2,1)S(1)} %copy-done.2, bf16[64,8,2,128]{3,2,1,0:T(2,128)(2,1)S(1)} %bitcast.64), kind=kOutput, calls=%fused_computation.4 | convolution fusion | flops 1074790400 | bytes 6553600 | tf_op jit(solution)/shard_map/dot_general | solution.py:86
  145.6 0.0 reduce-scatter.3.cloned.1.call-update
  145.7 0.0 copy-start.7
  145.7 42.3 %reduce-scatter.5.cloned.1.call-done = bf16[768,1024]{1,0:T(8,128)(2,1)} async-done(((bf16[768,4096]{1,0:T(8,128)(2,1)}), bf16[768,1024]{1,0:T(8,128)(2,1)}) %reduce-scatter.5.cloned.1.call-update) | async-done | bytes 1572880 | tf_op jit(solution)/shard_map/reduce_scatter | solution.py:123
  188.0 5.5 %all-to-all-start.1 = ((bf16[8,96,1024]{2,1,0:T(8,128)(2,1)}), bf16[8,96,1024]{2,1,0:T(8,128)(2,1)}, u32[]{:S(2)}, u32[]{:S(2)}) async-start(bf16[8,96,1024]{2,1,0:T(8,128)(2,1)} %bitcast.63), calls=%async_computation.3 | async-start | bytes 3145728 | tf_op jit(solution)/shard_map/all_to_all | solution.py:126
  193.5 0.1 reduce_sum.42
  193.6 0.1 copy.48
  193.7 0.1 copy.49
  193.9 0.1 copy.51
  194.0 36.5 %all-to-all-done.1 = bf16[8,96,1024]{2,1,0:T(8,128)(2,1)} async-done(((bf16[8,96,1024]{2,1,0:T(8,128)(2,1)}), bf16[8,96,1024]{2,1,0:T(8,128)(2,1)}, u32[]{:S(2)}, u32[]{:S(2)}) %all-to-all-start.1) | async-done | bytes 1572896 | tf_op jit(solution)/shard_map/all_to_all | solution.py:126
  230.4 4.3 %gather_fusion.1 = bf16[512,1024]{1,0:T(8,128)(2,1)S(1)} fusion(bf16[768,1024]{1,0:T(8,128)(2,1)} %bitcast.16, s32[1024]{0:T(1024)S(1)} %pad_clamp_fusion), kind=kCustom, calls=%fused_computation.1 | custom fusion | bytes 2099200 | tf_op jit(solution)/shard_map/jit(_take)/gather | solution.py:133
  234.8 1.2 gather.15
  236.0 3.6 %multiply_reduce_fusion = bf16[128,1024]{1,0:T(8,128)(2,1)} fusion(f32[128,4]{1,0:T(8,128)S(1)} %copy.51, bf16[128,4,1024]{2,1,0:T(4,128)(2,1)} %gather.15, pred[128,4]{1,0:T(8,128)(4,1)S(1)} %copy.49), kind=kLoop, calls=%fused_computation.11 | loop fusion | flops 1966080 | bytes 1313280 | tf_op jit(solution)/shard_map/reduce_sum | solution.py:135
  (34 shorter events, 0.2 us)
Async XLA Ops:
  7.2 110.1 %copy-start = (bf16[1,256,4096]{2,1,0:T(8,128)(2,1)S(1)}, bf16[1,256,4096]{2,1,0:T(8,128)(2,1)}, u32[]{:S(2)}) copy-start(bf16[1,256,4096]{2,1,0:T(8,128)(2,1)} %param.23) | copy-start | bytes 6291460
  7.2 3.0 %copy-start.1 = (bf16[128,4096]{1,0:T(8,128)(2,1)S(1)}, bf16[128,4096]{1,0:T(8,128)(2,1)}, u32[]{:S(2)}) copy-start(bf16[128,4096]{1,0:T(8,128)(2,1)} %param.17) | copy-start | bytes 3145732
  7.2 104.8 %all-gather.2.cloned.1.call-start = ((), (), s32[]{:S(2)}) async-start(), calls=%async_computation.5 | async-start | bytes 7864320 | tf_op jit(solution)/shard_map/all_gather | solution.py:115
  7.2 3.2 %copy-start.6 = (s32[128,4]{0,1:T(4,128)S(1)}, s32[128,4]{0,1:T(4,128)}, u32[]{:S(2)}) copy-start(s32[128,4]{0,1:T(4,128)} %param.19) | copy-start | bytes 6148
  66.5 121.5 %reduce-scatter.5.cloned.1.call-start = ((), (), s32[]{:S(2)}) async-start(), calls=%async_computation.6 | async-start | bytes 7864320 | tf_op jit(solution)/shard_map/reduce_scatter | solution.py:123
  129.9 0.8 copy-start.3
  129.9 4.2 %copy-start.4 = (bf16[256,128]{1,0:T(8,128)(2,1)S(1)}, bf16[256,128]{1,0:T(8,128)(2,1)}, u32[]{:S(2)}) copy-start(bf16[256,128]{1,0:T(8,128)(2,1)} %param.14) | copy-start | bytes 196612
  129.9 8.5 %copy-start.5 = (bf16[256,512]{1,0:T(8,128)(2,1)S(1)}, bf16[256,512]{1,0:T(8,128)(2,1)}, u32[]{:S(2)}) copy-start(bf16[256,512]{1,0:T(8,128)(2,1)} %param.12) | copy-start | bytes 786436
  129.9 8.9 %copy-start.8 = (f32[8]{0:T(128)S(1)}, f32[8]{0:T(128)}, u32[]{:S(2)}) copy-start(f32[8]{0:T(128)} %param.15) | copy-start | bytes 100
  130.0 109.7 %reduce-scatter.3.cloned.1.call-start = ((), (), s32[]{:S(2)}) async-start(), calls=%async_computation.4 | async-start | bytes 2621440 | tf_op jit(solution)/shard_map/reduce_scatter | solution.py:85
  130.8 8.2 %collective-permute-start.1 = (bf16[128,128]{1,0:T(8,128)(2,1)S(1)}, bf16[128,128]{1,0:T(8,128)(2,1)S(1)}, u32[]{:S(2)}, u32[]{:S(2)}) collective-permute-start(bf16[128,128]{1,0:T(8,128)(2,1)S(1)} %slice.20), channel_id=1, source_target_pairs={{0,4},{4,8},{8,12},{12,16},{16,20},{20,24},{24,28},{1,5},{5,9},{9,... | collective-permute-start | bytes 98312 | tf_op jit(solution)/shard_map/ppermute | solution.py:20
  134.2 5.1 %collective-permute-start = (bf16[128,128]{1,0:T(8,128)(2,1)S(1)}, bf16[128,128]{1,0:T(8,128)(2,1)S(1)}, u32[]{:S(2)}, u32[]{:S(2)}) collective-permute-start(bf16[128,128]{1,0:T(8,128)(2,1)S(1)} %slice.18), channel_id=1, source_target_pairs={{0,4},{4,8},{8,12},{12,16},{16,20},{20,24},{24,28},{1,5},{5,9},{9,... | collective-permute-start | bytes 98312 | tf_op jit(solution)/shard_map/ppermute | solution.py:20
  140.5 2.5 %copy-start.2 = (bf16[512,4096]{1,0:T(8,128)(2,1)S(1)}, bf16[512,4096]{1,0:T(8,128)(2,1)}, u32[]{:S(2)}) copy-start(bf16[512,4096]{1,0:T(8,128)(2,1)} %param.16) | copy-start | bytes 12582916
  145.7 48.2 %copy-start.7 = (f32[128,4]{0,1:T(4,128)S(1)}, f32[128,4]{0,1:T(4,128)}, u32[]{:S(2)}) copy-start(f32[128,4]{0,1:T(4,128)} %param.20) | copy-start | bytes 6148
  188.0 42.4 %all-to-all-start.1 = ((bf16[8,96,1024]{2,1,0:T(8,128)(2,1)}), bf16[8,96,1024]{2,1,0:T(8,128)(2,1)}, u32[]{:S(2)}, u32[]{:S(2)}) async-start(bf16[8,96,1024]{2,1,0:T(8,128)(2,1)} %bitcast.63), calls=%async_computation.3 | async-start | bytes 3145728 | tf_op jit(solution)/shard_map/all_to_all | solution.py:126
Sparse Core Ops, SparseCore 0:
  66.6 45.3 all-gather.1
  130.1 57.8 reduce-scatter.4
  191.1 31.1 reduce-scatter.2
where the time goes:
time: 247 us; the launch traced here: 246 us
  waiting for transfers between devices  124 us (50%)
  blocking collectives  44.2 us (18%)
  matrix products  21.6 us (9%)
  local copies, waits for them, and re-layouts  17.5 us (7%)
  between operations  14.1 us (6%)
  starting transfers between devices  12.6 us (5%)
  other arithmetic  11.9 us (5%)
    all_gather x1, waiting for transfers between devices, shards(): portion = lax.all_gather(arrived, 'tp', axis=1, tiled=True)  45.5 us
    all_to_all x1, blocking collectives, shards(): lax.all_to_all(outgoing, 'ep', split_axis=0, concat_axis=0, tiled=True)  44.2 us
    reduce_scatter x1, waiting for transfers between devices, shards(): lax.psum_scatter(partial_value.astype(jnp.bfloat16), 'tp', scatter_dimens...  42.3 us
    all_to_all x1, waiting for transfers between devices, shards(): lax.all_to_all(expert_result.reshape(experts, capacity, col_share), 'ep',...  36.5 us
    dot_general x1, matrix products, shards(): jnp.dot(activated, down_weight[0], preferred_element_type=jnp.float32)  12.7 us
    ppermute x2, starting transfers between devices, passed_along(): return lax.ppermute(block, axis, route)  6.93 us
    gather x2, local copies, waits for them, and re-layouts, shards(): jnp.take(returned.reshape(experts * capacity, col_share), target, axis=0)  5.57 us
    all_to_all x1, starting transfers between devices, shards(): lax.all_to_all(expert_result.reshape(experts, capacity, col_share), 'ep',...  5.51 us
  transfers between devices with their start and end apart: 6, of which 3 were waited for; matrix products, arithmetic and copies ran while one was open for 6% of the time, Pallas kernels for 0%

commit v1 on v0

--- a/solution.py
+++ b/solution.py
@@ -1,6 +1,8 @@
 import jax
 import jax.numpy as jnp
 from jax import lax
+from jax.experimental import pallas as pl
+from jax.experimental.pallas import tpu as pltpu
 from jax.sharding import PartitionSpec as P
 
 D = 4096
@@ -18,6 +20,463 @@
     devices = range(lax.axis_size(axis))
     route = [(i - distance, i) for i in devices if i - distance in devices]
     return lax.ppermute(block, axis, route)
+
+
+LINE = 4
+MESH = pl.DeviceIdType.MESH
+
+
+def chosen(z, values):
+    result = jnp.int32(values[0])
+    for place in range(1, LINE):
+        result = jnp.where(z == place, jnp.int32(values[place]), result)
+    return result
+
+
+def nearest_first(place):
+    return sorted(range(LINE), key=lambda other: (abs(other - place), other))
+
+
+def expert_kernel(
+    own_ref,
+    share_ref,
+    gate_ref,
+    up_ref,
+    down_ref,
+    out_ref,
+    rows_ref,
+    weight_ref,
+    sum_ref,
+    core_ref,
+    pair_ref,
+    side_ref,
+    up_line_ref,
+    down_line_ref,
+    last_ref,
+    share_send,
+    share_recv,
+    line_send,
+    line_recv,
+    side_send,
+    side_recv,
+    pair_send,
+    pair_recv,
+    core_send,
+    core_recv,
+    back_core_send,
+    back_core_recv,
+    back_pair_send,
+    back_pair_recv,
+    back_side_send,
+    back_side_recv,
+    back_line_send,
+    back_line_recv,
+    last_send,
+    last_recv,
+):
+    e, t = lax.axis_index("ep"), lax.axis_index("tp")
+    z, x, y, c = e // 2, e % 2, t // 2, t % 2
+    width = own_ref.shape[1]
+    tokens = own_ref.shape[0]
+    sibling, partner, beside = (e, y * 2 + 1 - c), (e, (1 - y) * 2 + c), (z * 2 + 1 - x, t)
+    above, below = (e + 2, t), (e - 2, t)
+
+    def copy(src, dst, send, recv, to):
+        return pltpu.make_async_remote_copy(
+            src_ref=src, dst_ref=dst, send_sem=send, recv_sem=recv, device_id=to, device_id_type=MESH
+        )
+
+    barrier = pltpu.get_barrier_semaphore()
+    for step in range(1, 2 * LINE):
+        pl.semaphore_signal(
+            barrier, inc=1, device_id=((e + step) % (2 * LINE), t), device_id_type=MESH
+        )
+    for other in (sibling, partner):
+        pl.semaphore_signal(barrier, inc=1, device_id=other, device_id_type=MESH)
+    pl.semaphore_wait(barrier, 2 * LINE + 1)
+
+    lone = width * 3 // 16
+    both = width // 8
+    first = pl.multiple_of(y * (width - 2 * lone) + c * lone, 128)
+    middle = pl.multiple_of(2 * lone + c * both, 128)
+    other_first = pl.multiple_of((1 - y) * (width - 2 * lone) + c * lone, 128)
+    parts = (pl.ds(first, lone), pl.ds(middle, both), pl.ds(other_first, lone))
+
+    def view(block, part):
+        return rows_ref.at[block, :, parts[part]]
+
+    def source(block, part, mine):
+        return own_ref.at[:, parts[part]] if mine else view(block, part)
+
+    def along(way, at, part, mine, to):
+        block = at * 2 + x
+        return copy(
+            source(block, part, mine), view(block, part),
+            line_send.at[way, at, part], line_recv.at[at, part], to,
+        )
+
+    def across(at, part, mine):
+        block = at * 2 + x
+        return copy(
+            source(block, part, mine), view(block, part),
+            side_send.at[at, part], side_recv.at[at, part], beside,
+        )
+
+    def across_in(at, part):
+        block = at * 2 + 1 - x
+        return copy(
+            view(block, part), view(block, part), side_send.at[at, part], side_recv.at[at, part], beside
+        )
+
+    def to_partner(block):
+        return copy(view(block, 0), view(block, 0), pair_send.at[block], pair_recv.at[block], partner)
+
+    def from_partner(block):
+        return copy(view(block, 2), view(block, 2), pair_send.at[block], pair_recv.at[block], partner)
+
+    def to_sibling(block, part):
+        return copy(
+            view(block, part), view(block, part), core_send.at[block, part], core_recv.at[block, part], sibling
+        )
+
+    sibling_parts = (
+        pl.ds(pl.multiple_of(y * (width - 2 * lone) + (1 - c) * lone, 128), lone),
+        pl.ds(pl.multiple_of(2 * lone + (1 - c) * both, 128), both),
+        pl.ds(pl.multiple_of((1 - y) * (width - 2 * lone) + (1 - c) * lone, 128), lone),
+    )
+
+    def from_sibling(block, part):
+        dst = rows_ref.at[block, :, sibling_parts[part]]
+        return copy(dst, dst, core_send.at[block, part], core_recv.at[block, part], sibling)
+
+    def share_copy(step):
+        to = (e + step) % (2 * LINE)
+        return copy(
+            share_ref.at[to], weight_ref.at[e], share_send.at[step], share_recv.at[e], (to, t)
+        )
+
+    def share_in(step):
+        at = (e + step) % (2 * LINE)
+        return copy(share_ref.at[at], weight_ref.at[at], share_send.at[step], share_recv.at[at], (at, t))
+
+    for part in (0, 1):
+        @pl.when(z < LINE - 1)
+        def _():
+            along(0, z, part, True, above).start()
+
+        @pl.when(z > 0)
+        def _():
+            along(1, z, part, True, below).start()
+
+        across(z, part, True).start()
+    for step in range(1, 2 * LINE):
+        share_copy(step).start()
+    rows_ref[e] = own_ref[...]
+    weight_ref[e] = share_ref[e]
+
+    near = [chosen(z, [nearest_first(place)[j] for place in range(LINE)]) for j in range(LINE)]
+    sequence = []
+
+    def passed_on(block):
+        to_partner(block).start()
+        to_sibling(block, 0).start()
+        to_sibling(block, 1).start()
+        sequence.append(block)
+
+    def settle(block):
+        from_partner(block).wait_recv()
+        to_sibling(block, 2).start()
+
+    for j in range(1, LINE + 1):
+        if j < LINE:
+            at = near[j]
+            for part in (0, 1):
+                along(0, at, part, False, above).wait_recv()
+
+                @pl.when((at < z) & (z < LINE - 1))
+                def _():
+                    along(0, at, part, False, above).start()
+
+                @pl.when((at > z) & (z > 0))
+                def _():
+                    along(1, at, part, False, below).start()
+
+                across(at, part, False).start()
+            passed_on(at * 2 + x)
+            if len(sequence) > 2:
+                settle(sequence[len(sequence) - 3])
+        for part in (0, 1):
+            across_in(near[j - 1], part).wait_recv()
+        passed_on(near[j - 1] * 2 + 1 - x)
+        if len(sequence) > 2:
+            settle(sequence[len(sequence) - 3])
+    for block in sequence[-2:]:
+        settle(block)
+    for step in range(1, 2 * LINE):
+        share_in(step).wait_recv()
+    for block in sequence:
+        for part in range(3):
+            from_sibling(block, part).wait_recv()
+
+    quarter = width // 4
+    early = quarter * 5 // 8
+    late = quarter - early
+    mine = pl.multiple_of((y * 2 + c) * quarter, 128)
+    theirs = pl.multiple_of(((1 - y) * 2 + c) * quarter, 128)
+    early_mine, early_theirs = pl.ds(mine, early), pl.ds(theirs, early)
+    late_mine = pl.ds(pl.multiple_of(mine + early, 128), late)
+    late_theirs = pl.ds(pl.multiple_of(theirs + early, 128), late)
+    own_quarter, other_quarter = pl.ds(mine, quarter), pl.ds(theirs, quarter)
+    sent_quarters = [
+        pl.ds(pl.multiple_of((half * 2 + 1 - c) * quarter, 128), quarter) for half in range(2)
+    ]
+    kept_quarters = [
+        pl.ds(pl.multiple_of((half * 2 + c) * quarter, 128), quarter) for half in range(2)
+    ]
+    trio = ((early_mine, 0, early), (late_mine, early, late), (late_theirs, quarter, late))
+
+    def add(block, columns, arrived):
+        total = sum_ref[block, :, columns].astype(jnp.float32)
+        sum_ref[block, :, columns] = (total + arrived.astype(jnp.float32)).astype(jnp.bfloat16)
+
+    def far(j):
+        result = chosen(z, [nearest_first(place)[::-1][0] for place in range(LINE)])
+        for index in range(1, LINE):
+            value = chosen(z, [nearest_first(place)[::-1][index] for place in range(LINE)])
+            result = jnp.where(j == index, value, result)
+        return result
+
+    def back_core(block, half, columns):
+        return copy(
+            sum_ref.at[block, :, columns], core_ref.at[block, :, pl.ds(half * quarter, quarter)],
+            back_core_send.at[block, half], back_core_recv.at[block, half], sibling,
+        )
+
+    def back_pair(block):
+        return copy(
+            sum_ref.at[block, :, early_theirs], pair_ref.at[block],
+            back_pair_send.at[block], back_pair_recv.at[block], partner,
+        )
+
+    def back_side(at, index):
+        columns, start, length = trio[index]
+        return copy(
+            sum_ref.at[at * 2 + 1 - x, :, columns], side_ref.at[at, :, pl.ds(start, length)],
+            back_side_send.at[at, index], back_side_recv.at[at, index], beside,
+        )
+
+    def back_line(way, at, index, to):
+        columns, start, length = trio[index]
+        landing = (up_line_ref, down_line_ref)[way]
+        return copy(
+            sum_ref.at[at * 2 + x, :, columns], landing.at[at, :, pl.ds(start, length)],
+            back_line_send.at[at, index], back_line_recv.at[way, at, index], to,
+        )
+
+    def line_in(way, at):
+        for index, (columns, start, length) in enumerate(trio):
+            back_line(way, at, index, above).wait_recv()
+            landing = (up_line_ref, down_line_ref)[way]
+            add(at * 2 + x, columns, landing[at, :, start : start + length])
+
+    last = copy(sum_ref.at[e, :, late_theirs], last_ref, last_send, last_recv, partner)
+
+    def experts_of(block):
+        rows = rows_ref[block]
+        gate_pre = jnp.dot(rows, gate_ref[...], preferred_element_type=jnp.float32)
+        up_pre = jnp.dot(rows, up_ref[...], preferred_element_type=jnp.float32)
+        gate_cut = jnp.minimum(gate_pre, CLAMP)
+        activated = (
+            (jnp.clip(up_pre, -CLAMP, CLAMP) + 1.0) * gate_cut * jax.nn.sigmoid(SLOPE * gate_cut)
+        ).astype(jnp.bfloat16)
+        weight = jnp.broadcast_to(weight_ref[block][0:1], (tokens, tokens)).T[:, 0:1]
+
+        for place in range(0, width, quarter):
+            result = jnp.dot(
+                activated, down_ref[:, place : place + quarter], preferred_element_type=jnp.float32
+            )
+            sum_ref[block, :, place : place + quarter] = (result * weight).astype(jnp.bfloat16)
+
+    def turn(i, carry):
+        @pl.when(i < LINE)
+        def _():
+            at = far(i)
+
+            def one(index, inner):
+                block = at * 2 + (1 - x) * (1 - index) + x * index
+                experts_of(block)
+                for half in range(2):
+                    back_core(block, half, sent_quarters[half]).start()
+                return inner
+
+            lax.fori_loop(0, 2, one, 0)
+
+        @pl.when((i >= 1) & (i < LINE + 1))
+        def _():
+            at = far(i - 1)
+
+            def one(index, inner):
+                block = at * 2 + (1 - x) * (1 - index) + x * index
+                for half in range(2):
+                    back_core(block, half, sent_quarters[half]).wait_recv()
+                    add(block, kept_quarters[half], core_ref[block, :, half * quarter : (half + 1) * quarter])
+                back_pair(block).start()
+                return inner
+
+            lax.fori_loop(0, 2, one, 0)
+
+        @pl.when((i >= 2) & (i < LINE + 2))
+        def _():
+            at = far(i - 2)
+
+            def one(index, inner):
+                block = at * 2 + (1 - x) * (1 - index) + x * index
+                back_pair(block).wait_recv()
+                add(block, early_mine, pair_ref[block])
+
+                @pl.when(index == 0)
+                def _():
+                    for part in range(3):
+                        back_side(at, part).start()
+
+                return inner
+
+            lax.fori_loop(0, 2, one, 0)
+
+        @pl.when(i >= 3)
+        def _():
+            at = far(i - 3)
+            for part, (columns, start, length) in enumerate(trio):
+                back_side(at, part).wait_recv()
+                add(at * 2 + x, columns, side_ref[at, :, start : start + length])
+
+            @pl.when((at >= z) & (z > 0))
+            def _():
+                line_in(0, at)
+
+            @pl.when((at <= z) & (z < LINE - 1))
+            def _():
+                line_in(1, at)
+
+            @pl.when(at > z)
+            def _():
+                for part in range(3):
+                    back_line(0, at, part, above).start()
+
+            @pl.when(at < z)
+            def _():
+                for part in range(3):
+                    back_line(1, at, part, below).start()
+
+        return carry
+
+    lax.fori_loop(0, LINE + 3, turn, 0)
+    last.start()
+    last.wait_recv()
+    out_ref[:, 0:early] = sum_ref[e, :, early_mine]
+    closing = sum_ref[e, :, late_mine].astype(jnp.float32) + last_ref[...].astype(jnp.float32)
+    out_ref[:, early:quarter] = closing.astype(jnp.bfloat16)
+
+    last.wait_send()
+    for part in (0, 1):
+        @pl.when(z < LINE - 1)
+        def _():
+            along(0, z, part, True, above).wait_send()
+
+        @pl.when(z > 0)
+        def _():
+            along(1, z, part, True, below).wait_send()
+
+        across(z, part, True).wait_send()
+    for step in range(1, 2 * LINE):
+        share_copy(step).wait_send()
+    for j in range(1, LINE):
+        at = near[j]
+        for part in (0, 1):
+            @pl.when((at < z) & (z < LINE - 1))
+            def _():
+                along(0, at, part, False, above).wait_send()
+
+            @pl.when((at > z) & (z > 0))
+            def _():
+                along(1, at, part, False, below).wait_send()
+
+            across(at, part, False).wait_send()
+    for block in sequence:
+        to_partner(block).wait_send()
+        for part in range(3):
+            to_sibling(block, part).wait_send()
+
+    def drained(at, carry):
+        for side in range(2):
+            for half in range(2):
+                back_core(at * 2 + side, half, sent_quarters[half]).wait_send()
+            back_pair(at * 2 + side).wait_send()
+        for part in range(3):
+            back_side(at, part).wait_send()
+
+            @pl.when(at != z)
+            def _():
+                back_line(0, at, part, above).wait_send()
+
+        return carry
+
+    lax.fori_loop(0, LINE, drained, 0)
+
+
+def expert_call(normed, share_of, gate_one, up_one, down_one):
+    tokens, width = normed.shape
+    quarter = width // 4
+    early = quarter * 5 // 8
+    carried = quarter + quarter - early
+    blocks = 2 * LINE
+    kept = jnp.bfloat16
+    dma = pltpu.SemaphoreType.DMA
+    return pl.pallas_call(
+        expert_kernel,
+        out_shape=jax.ShapeDtypeStruct((tokens, quarter), jnp.bfloat16),
+        in_specs=[pl.BlockSpec(memory_space=pltpu.VMEM)] * 5,
+        out_specs=pl.BlockSpec(memory_space=pltpu.VMEM),
+        scratch_shapes=[
+            pltpu.VMEM((blocks, tokens, width), kept),
+            pltpu.VMEM((blocks, 8, tokens), jnp.float32),
+            pltpu.VMEM((blocks, tokens, width), kept),
+            pltpu.VMEM((blocks, tokens, 2 * quarter), kept),
+            pltpu.VMEM((blocks, tokens, early), kept),
+            pltpu.VMEM((LINE, tokens, carried), kept),
+            pltpu.VMEM((LINE, tokens, carried), kept),
+            pltpu.VMEM((LINE, tokens, carried), kept),
+            pltpu.VMEM((tokens, quarter - early), kept),
+            dma((blocks,)),
+            dma((blocks,)),
+            dma((2, LINE, 2)),
+            dma((LINE, 2)),
+            dma((LINE, 2)),
+            dma((LINE, 2)),
+            dma((blocks,)),
+            dma((blocks,)),
+            dma((blocks, 3)),
+            dma((blocks, 3)),
+            dma((blocks, 2)),
+            dma((blocks, 2)),
+            dma((blocks,)),
+            dma((blocks,)),
+            dma((LINE, 3)),
+            dma((LINE, 3)),
+            dma((LINE, 3)),
+            dma((2, LINE, 3)),
+            dma,
+            dma,
+        ],
+        compiler_params=pltpu.CompilerParams(
+            collective_id=0, has_side_effects=True, vmem_limit_bytes=60 * 1024 * 1024
+        ),
+        cost_estimate=pl.CostEstimate(
+            flops=6 * blocks * tokens * width * gate_one.shape[1],
+            bytes_accessed=8 * width * gate_one.shape[1],
+            transcendentals=0,
+        ),
+    )(normed, share_of, gate_one, up_one, down_one)
 
 
 def shards(
@@ -98,41 +557,49 @@
         * lax.rsqrt(jnp.mean(widened * widened, axis=-1, keepdims=True) + EPS)
         * norm_gain[None, :]
     ).astype(jnp.bfloat16)
-    flat_ids = routing.reshape(-1)
-    onehot = (flat_ids[:, None] == jnp.arange(experts, dtype=jnp.int32)[None, :]).astype(jnp.int32)
-    rank_in = jnp.cumsum(onehot, axis=0) - 1
-    target = flat_ids * capacity + jnp.sum(rank_in * onehot, axis=1)
-    tok_ids = jnp.arange(token_rows * TOPK) // TOPK
-    slot_tok = jnp.full((experts * capacity,), token_rows, jnp.int32).at[target].set(tok_ids)
-    gate_one = gate_weight[0]
-    up_one = up_weight[0]
-    own_cols = lax.dynamic_slice_in_dim(normed, lax.axis_index("tp") * col_share, col_share, 1)
-    extended = jnp.concatenate([own_cols, jnp.zeros((1, col_share), jnp.bfloat16)], axis=0)
-    outgoing = jnp.take(extended, slot_tok, axis=0).reshape(experts, capacity, col_share)
-    arrived = lax.all_to_all(outgoing, "ep", split_axis=0, concat_axis=0, tiled=True).reshape(
-        experts * capacity, col_share
-    )
-    portion = lax.all_gather(arrived, "tp", axis=1, tiled=True)
-    gate_pre = jnp.dot(portion, gate_one, preferred_element_type=jnp.float32)
-    up_pre = jnp.dot(portion, up_one, preferred_element_type=jnp.float32)
-    gate_cut = jnp.minimum(gate_pre, CLAMP)
-    activated = (
-        (jnp.clip(up_pre, -CLAMP, CLAMP) + 1.0) * gate_cut * jax.nn.sigmoid(SLOPE * gate_cut)
-    ).astype(jnp.bfloat16)
-    partial_value = jnp.dot(activated, down_weight[0], preferred_element_type=jnp.float32)
-    expert_result = lax.psum_scatter(
-        partial_value.astype(jnp.bfloat16), "tp", scatter_dimension=1, tiled=True
-    )
-    returned = lax.all_to_all(
-        expert_result.reshape(experts, capacity, col_share),
-        "ep",
-        split_axis=0,
-        concat_axis=0,
-        tiled=True,
-    )
-    picked = jnp.take(returned.reshape(experts * capacity, col_share), target, axis=0)
-    picked = picked.astype(jnp.float32).reshape(token_rows, TOPK, col_share)
-    expert_output = jnp.sum(picked * route_weight[:, :, None], axis=1).astype(jnp.bfloat16)
+    if (experts, lax.axis_size("tp")) != (2 * LINE, 4) or token_rows % 16:
+        flat_ids = routing.reshape(-1)
+        onehot = (flat_ids[:, None] == jnp.arange(experts, dtype=jnp.int32)[None, :]).astype(jnp.int32)
+        rank_in = jnp.cumsum(onehot, axis=0) - 1
+        target = flat_ids * capacity + jnp.sum(rank_in * onehot, axis=1)
+        tok_ids = jnp.arange(token_rows * TOPK) // TOPK
+        slot_tok = jnp.full((experts * capacity,), token_rows, jnp.int32).at[target].set(tok_ids)
+        gate_one = gate_weight[0]
+        up_one = up_weight[0]
+        own_cols = lax.dynamic_slice_in_dim(normed, lax.axis_index("tp") * col_share, col_share, 1)
+        extended = jnp.concatenate([own_cols, jnp.zeros((1, col_share), jnp.bfloat16)], axis=0)
+        outgoing = jnp.take(extended, slot_tok, axis=0).reshape(experts, capacity, col_share)
+        arrived = lax.all_to_all(outgoing, "ep", split_axis=0, concat_axis=0, tiled=True).reshape(
+            experts * capacity, col_share
+        )
+        portion = lax.all_gather(arrived, "tp", axis=1, tiled=True)
+        gate_pre = jnp.dot(portion, gate_one, preferred_element_type=jnp.float32)
+        up_pre = jnp.dot(portion, up_one, preferred_element_type=jnp.float32)
+        gate_cut = jnp.minimum(gate_pre, CLAMP)
+        activated = (
+            (jnp.clip(up_pre, -CLAMP, CLAMP) + 1.0) * gate_cut * jax.nn.sigmoid(SLOPE * gate_cut)
+        ).astype(jnp.bfloat16)
+        partial_value = jnp.dot(activated, down_weight[0], preferred_element_type=jnp.float32)
+        expert_result = lax.psum_scatter(
+            partial_value.astype(jnp.bfloat16), "tp", scatter_dimension=1, tiled=True
+        )
+        returned = lax.all_to_all(
+            expert_result.reshape(experts, capacity, col_share),
+            "ep",
+            split_axis=0,
+            concat_axis=0,
+            tiled=True,
+        )
+        picked = jnp.take(returned.reshape(experts * capacity, col_share), target, axis=0)
+        picked = picked.astype(jnp.float32).reshape(token_rows, TOPK, col_share)
+        expert_output = jnp.sum(picked * route_weight[:, :, None], axis=1).astype(jnp.bfloat16)
+    else:
+        named = routing == lax.broadcasted_iota(jnp.int32, (experts, 1, 1), 0)
+        share_of = jnp.sum(jnp.where(named, route_weight[None], 0.0), axis=2)
+        share_of = jnp.broadcast_to(share_of[:, None, :], (experts, 8, token_rows))
+        expert_output = expert_call(
+            normed, share_of, gate_weight[0], up_weight[0], down_weight[0]
+        )
     return (mixer_output, expert_output)
 
 

time: 247 us -> 155 us (0.63)
  waiting for transfers between devices: 124 us -> 0.04 us
  Pallas kernels: 0 us -> 113 us
  blocking collectives: 44.2 us -> 0 us
  matrix products: 21.6 us -> 3.68 us
  other arithmetic: 11.9 us -> 3.27 us
  local copies, waits for them, and re-layouts: 17.5 us -> 11.2 us
  starting transfers between devices: 12.6 us -> 8.34 us
    pallas_call x0 -> x1, Pallas kernels: none -> 113 us  [expert_call(): pl.pallas_call(expert_kernel, out_shape=jax.ShapeDtypeStruct((tokens, qua...]
    all_gather x1 -> x0, waiting for transfers between devices: 45.5 us -> none  [shards(): portion = lax.all_gather(arrived, 'tp', axis=1, tiled=True)]
    all_to_all x1 -> x0, blocking collectives: 44.2 us -> none  [shards(): lax.all_to_all(outgoing, 'ep', split_axis=0, concat_axis=0, tiled=True)]
    reduce_scatter x1 -> x0, waiting for transfers between devices: 42.3 us -> none  [shards(): lax.psum_scatter(partial_value.astype(jnp.bfloat16), 'tp', scatter_dimens...]
    all_to_all x1 -> x0, waiting for transfers between devices: 36.5 us -> none  [shards(): lax.all_to_all(expert_result.reshape(experts, capacity, col_share), 'ep',...]
    dot_general x2 -> x0, matrix products: 17.9 us -> none  [the longest x1 12.7 us: shards(): jnp.dot(activated, down_weight[0], preferred_element_type=jnp.float32)]
    gather x3 -> x0, local copies, waits for them, and re-layouts: 9.14 us -> none  [the longest x2 5.57 us: shards(): jnp.take(returned.reshape(experts * capacity, col_share), target, axis=0)]
    all_to_all x1 -> x0, starting transfers between devices: 5.51 us -> none  [shards(): lax.all_to_all(expert_result.reshape(experts, capacity, col_share), 'ep',...]
  transfers between devices with their start and end apart: 6 -> 3, of which waited for: 3 -> 0; matrix products, arithmetic and copies ran while one was open for 6% -> 6% of each run, Pallas kernels for 0% -> 74%
where the time goes in v1:
time: 155 us; the launch traced here: 154 us
  Pallas kernels  113 us (73%)
  between operations  14.2 us (9%)
  local copies, waits for them, and re-layouts  11.2 us (7%)
  starting transfers between devices  8.34 us (5%)
  matrix products  3.68 us (2%)
  other arithmetic  3.27 us (2%)
    pallas_call x1, Pallas kernels, expert_call(): pl.pallas_call(expert_kernel, out_shape=jax.ShapeDtypeStruct((tokens, qua...  113 us
    ppermute x2, starting transfers between devices, passed_along(): return lax.ppermute(block, axis, route)  8.3 us
    unnamed x13, local copies, waits for them, and re-layouts  4.32 us
  transfers between devices with their start and end apart: 3, of which 0 were waited for; matrix products, arithmetic and copies ran while one was open for 6% of the time, Pallas kernels for 74%

profile of v1, /device:TPU:0, one launch (start us, length us, event | category | flops | bytes accessed | tf_op | source)
XLA Modules:
  0.0 154.0 jit_solution(15389101093922779215)
XLA Ops:
  7.2 0.0 reduce-scatter.2.cloned.1.call-start
  7.2 0.8 slice.14
  8.0 4.9 %collective-permute-start.1 = (bf16[128,128]{1,0:T(8,128)(2,1)S(1)}, bf16[128,128]{1,0:T(8,128)(2,1)S(1)}, u32[]{:S(2)}, u32[]{:S(2)}) collective-permute-start(bf16[128,128]{1,0:T(8,128)(2,1)S(1)} %slice.14), channel_id=1, source_target_pairs={{0,4},{4,8},{8,12},{12,16},{16,20},{20,24},{24,28},{1,5},{5,9},{9,... | collective-permute-start | bytes 98312 | tf_op jit(solution)/shard_map/ppermute | solution.py:22
  12.8 0.8 slice.12
  13.6 3.4 %collective-permute-start = (bf16[128,128]{1,0:T(8,128)(2,1)S(1)}, bf16[128,128]{1,0:T(8,128)(2,1)S(1)}, u32[]{:S(2)}, u32[]{:S(2)}) collective-permute-start(bf16[128,128]{1,0:T(8,128)(2,1)S(1)} %slice.12), channel_id=1, source_target_pairs={{0,4},{4,8},{8,12},{12,16},{16,20},{20,24},{24,28},{1,5},{5,9},{9,... | collective-permute-start | bytes 98312 | tf_op jit(solution)/shard_map/ppermute | solution.py:22
  17.1 0.1 iota_add_fusion
  17.1 0.1 broadcast_compare_fusion
  17.2 0.1 iota_add_fusion.1
  17.3 0.2 fusion.9
  17.5 0.9 reshape.141
  18.4 0.9 reshape.139
  19.4 1.3 reshape.142
  20.7 0.1 copy.39
  20.8 0.7 max.18
  21.5 0.1 copy.35
  21.6 0.0 collective-permute-done.1
  21.6 0.8 pad_maximum_fusion
  22.4 0.1 reshape.140
  22.5 0.1 copy.38
  22.6 0.0 copy-start.2
  22.6 0.5 fusion.16
  23.1 0.1 broadcast_maximum_fusion
  23.2 0.3 fusion.3
  23.5 0.1 exponential_add_fusion
  23.6 0.0 collective-permute-done
  23.6 0.0 copy-done.2
  23.6 0.1 reshape.138
  23.7 0.1 copy.34
  23.9 0.0 copy-start.1
  23.9 0.5 fusion.4
  24.4 0.3 copy.43
  24.6 1.4 copy-done.1
  26.1 2.7 %convolution_convert_fusion = bf16[256,4096]{1,0:T(8,128)(2,1)} fusion(bf16[512,4096]{1,0:T(8,128)(2,1)S(1)} %copy-done.1, bf16[64,8,2,128]{3,2,1,0:T(2,128)(2,1)S(1)} %bitcast.27), kind=kOutput, calls=%fused_computation | convolution fusion | flops 1074790400 | bytes 6553600 | tf_op jit(solution)/shard_map/dot_general | solution.py:545
  28.7 0.0 copy-start.4
  28.7 0.0 copy-start.5
  28.7 0.0 copy-start
  28.7 0.0 copy-start.3
  28.7 0.0 reduce-scatter.2.cloned.1.call-update
  28.8 0.6 copy-done.4
  29.4 0.0 copy-done.5
  29.4 0.6 copy-done
  30.0 0.3 fusion
  30.3 0.0 copy-done.3
  30.3 1.3 fusion.2.own_ref
  31.6 0.6 broadcast_in_dim.44.share_ref
  32.2 113.2 %shard_map.131 = bf16[128,1024]{1,0:T(8,128)(2,1)} custom-call(bf16[128,4096]{1,0:T(8,128)(2,1)} %fusion.2.own_ref, f32[8,8,128]{2,1,0:T(8,128)} %broadcast_in_dim.44.share_ref, bf16[4096,256]{1,0:T(8,128)(2,1)} %bitcast.28, bf16[4096,256]{1,0:T(8,128)(2,1)} %bitcast.29, bf16[256,4096]{1,0:T(8,128)(2,1)} %bitcast.30), custom_call_target="tpu_custom_call" | custom-call | flops 6442450944 | bytes 8388608 | tf_op jit(solution)/shard_map/pallas_call | solution.py:435
  145.4 0.0 reduce-scatter.2.cloned.1.call-done
  145.5 1.7 %copy.67 = bf16[128,1024]{1,0:T(8,128)(2,1)} copy(bf16[128,1024]{1,0:T(8,128)(2,1)} %shard_map.131) | data formatting | bytes 524288
  (4 shorter events, 0.0 us)
Async XLA Ops:
  7.2 138.3 %reduce-scatter.2.cloned.1.call-start = ((), (), s32[]{:S(2)}) async-start(), calls=%async_computation.1 | async-start | bytes 2621440 | tf_op jit(solution)/shard_map/reduce_scatter | solution.py:544
  8.0 13.6 %collective-permute-start.1 = (bf16[128,128]{1,0:T(8,128)(2,1)S(1)}, bf16[128,128]{1,0:T(8,128)(2,1)S(1)}, u32[]{:S(2)}, u32[]{:S(2)}) collective-permute-start(bf16[128,128]{1,0:T(8,128)(2,1)S(1)} %slice.14), channel_id=1, source_target_pairs={{0,4},{4,8},{8,12},{12,16},{16,20},{20,24},{24,28},{1,5},{5,9},{9,... | collective-permute-start | bytes 98312 | tf_op jit(solution)/shard_map/ppermute | solution.py:22
  13.6 10.0 %collective-permute-start = (bf16[128,128]{1,0:T(8,128)(2,1)S(1)}, bf16[128,128]{1,0:T(8,128)(2,1)S(1)}, u32[]{:S(2)}, u32[]{:S(2)}) collective-permute-start(bf16[128,128]{1,0:T(8,128)(2,1)S(1)} %slice.12), channel_id=1, source_target_pairs={{0,4},{4,8},{8,12},{12,16},{16,20},{20,24},{24,28},{1,5},{5,9},{9,... | collective-permute-start | bytes 98312 | tf_op jit(solution)/shard_map/ppermute | solution.py:22
  22.6 1.0 copy-start.2
  23.9 2.2 %copy-start.1 = (bf16[512,4096]{1,0:T(8,128)(2,1)S(1)}, bf16[512,4096]{1,0:T(8,128)(2,1)}, u32[]{:S(2)}) copy-start(bf16[512,4096]{1,0:T(8,128)(2,1)} %param.16) | copy-start | bytes 12582916
  28.7 0.7 copy-start.4
  28.7 0.7 copy-start.5
  28.7 1.3 copy-start
  28.7 1.5 %copy-start.3 = (f32[4096]{0:T(1024)S(1)}, f32[4096]{0:T(1024)}, u32[]{:S(2)}) copy-start(f32[4096]{0:T(1024)} %param.18) | copy-start | bytes 49156
Sparse Core Ops, SparseCore 0:
  28.9 42.2 reduce-scatter.1

commit v2 on v1

--- a/solution.py
+++ b/solution.py
@@ -37,13 +37,35 @@
     return sorted(range(LINE), key=lambda other: (abs(other - place), other))
 
 
-def expert_kernel(
+def layer_kernel(
     own_ref,
     share_ref,
+    gate_hbm,
+    up_hbm,
+    down_hbm,
+    query_ref,
+    key_ref,
+    value_ref,
+    sink_ref,
+    project_hbm,
+    mixer_ref,
+    out_ref,
     gate_ref,
     up_ref,
     down_ref,
-    out_ref,
+    project_ref,
+    halo_ref,
+    attended_ref,
+    mixed_ref,
+    mixed_core_ref,
+    mixed_pair_ref,
+    load_sem,
+    halo_send,
+    halo_recv,
+    mixed_core_send,
+    mixed_core_recv,
+    mixed_pair_send,
+    mixed_pair_recv,
     rows_ref,
     weight_ref,
     sum_ref,
@@ -86,6 +108,14 @@
             src_ref=src, dst_ref=dst, send_sem=send, recv_sem=recv, device_id=to, device_id_type=MESH
         )
 
+    loads = [
+        pltpu.make_async_copy(src, dst, load_sem.at[place])
+        for place, (src, dst) in enumerate(
+            [(project_hbm, project_ref), (gate_hbm, gate_ref), (up_hbm, up_ref), (down_hbm, down_ref)]
+        )
+    ]
+    for load in loads:
+        load.start()
     barrier = pltpu.get_barrier_semaphore()
     for step in range(1, 2 * LINE):
         pl.semaphore_signal(
@@ -169,11 +199,110 @@
             along(1, z, part, True, below).start()
 
         across(z, part, True).start()
+    queries = query_ref.shape[0]
+
+    def halo_copy(which):
+        src = (key_ref, value_ref)[which].at[pl.ds(queries - WINDOW_KEYS, WINDOW_KEYS)]
+        to = ((e + 1) % (2 * LINE), t)
+        return copy(src, halo_ref.at[which], halo_send.at[which], halo_recv.at[which], to)
+
+    @pl.when(e < 2 * LINE - 1)
+    def _():
+        halo_copy(0).start()
+        halo_copy(1).start()
+
+    @pl.when(e == 0)
+    def _():
+        halo_ref[...] = jnp.zeros_like(halo_ref)
+
     for step in range(1, 2 * LINE):
         share_copy(step).start()
     rows_ref[e] = own_ref[...]
     weight_ref[e] = share_ref[e]
 
+    kv_heads = key_ref.shape[1] // HEAD_SIZE
+    group = query_ref.shape[1] // HEAD_SIZE // kv_heads
+    span = queries // 4
+    here = lax.broadcasted_iota(jnp.int32, (WINDOW_KEYS, 2 * WINDOW_KEYS), 0)
+    there = lax.broadcasted_iota(jnp.int32, (WINDOW_KEYS, 2 * WINDOW_KEYS), 1)
+
+    def attend(number):
+        begin = number * WINDOW_KEYS
+        permitted = (there > here) & (there <= here + WINDOW_KEYS)
+        if number == 0:
+            permitted = permitted & ((there >= WINDOW_KEYS) | (e > 0))
+        for kv in range(kv_heads):
+            lanes = slice(kv * HEAD_SIZE, (kv + 1) * HEAD_SIZE)
+            if number == 0:
+                keys = jnp.concatenate([halo_ref[0][:, lanes], key_ref[0:WINDOW_KEYS, lanes]], axis=0)
+                values = jnp.concatenate(
+                    [halo_ref[1][:, lanes], value_ref[0:WINDOW_KEYS, lanes]], axis=0
+                )
+            else:
+                keys = key_ref[begin - WINDOW_KEYS : begin + WINDOW_KEYS, lanes]
+                values = value_ref[begin - WINDOW_KEYS : begin + WINDOW_KEYS, lanes]
+            for member in range(group):
+                head = kv * group + member
+                columns = slice(head * HEAD_SIZE, (head + 1) * HEAD_SIZE)
+                scores = lax.dot_general(
+                    query_ref[begin : begin + WINDOW_KEYS, columns],
+                    keys,
+                    (((1,), (1,)), ((), ())),
+                    preferred_element_type=jnp.float32,
+                ) * HEAD_SIZE ** (-0.5)
+                scores = jnp.where(permitted, scores, -jnp.inf)
+                sink = sink_ref[head]
+                highest = jnp.maximum(jnp.max(scores, axis=-1, keepdims=True), sink)
+                numerator = jnp.exp(scores - highest)
+                denominator = jnp.sum(numerator, axis=-1, keepdims=True) + jnp.exp(sink - highest)
+                weights = (numerator / denominator).astype(jnp.bfloat16)
+                found = jnp.dot(weights, values, preferred_element_type=jnp.float32)
+                attended_ref[begin : begin + WINDOW_KEYS, columns] = found.astype(jnp.bfloat16)
+
+    def mixed_core(half):
+        at = pl.multiple_of((half * 2 + 1 - c) * span, 16)
+        return copy(
+            mixed_ref.at[pl.ds(at, span)], mixed_core_ref.at[half],
+            mixed_core_send.at[half], mixed_core_recv.at[half], sibling,
+        )
+
+    mixed_pair = copy(
+        mixed_ref.at[pl.ds(pl.multiple_of(((1 - y) * 2 + c) * span, 16), span)], mixed_pair_ref,
+        mixed_pair_send, mixed_pair_recv, partner,
+    )
+
+    def mixed_rows(half):
+        return pl.ds(pl.multiple_of((half * 2 + c) * span, 16), span)
+
+    def mix():
+        for number in range(1, queries // WINDOW_KEYS):
+            attend(number)
+
+        @pl.when(e > 0)
+        def _():
+            halo_copy(0).wait_recv()
+            halo_copy(1).wait_recv()
+
+        attend(0)
+        loads[0].wait()
+        for place in range(0, width, width // 4):
+            columns = slice(place, place + width // 4)
+            mixed_ref[:, columns] = jnp.dot(
+                attended_ref[...], project_ref[:, columns], preferred_element_type=jnp.float32
+            ).astype(jnp.bfloat16)
+        for half in range(2):
+            mixed_core(half).start()
+
+    def mix_onward():
+        for half in range(2):
+            mixed_core(half).wait_recv()
+            total = mixed_ref[mixed_rows(half), :].astype(jnp.float32)
+            mixed_ref[mixed_rows(half), :] = (
+                total + mixed_core_ref[half].astype(jnp.float32)
+            ).astype(jnp.bfloat16)
+        mixed_pair.start()
+
+    mix()
     near = [chosen(z, [nearest_first(place)[j] for place in range(LINE)]) for j in range(LINE)]
     sequence = []
 
@@ -210,8 +339,11 @@
         passed_on(near[j - 1] * 2 + 1 - x)
         if len(sequence) > 2:
             settle(sequence[len(sequence) - 3])
+    mix_onward()
     for block in sequence[-2:]:
         settle(block)
+    for load in loads[1:]:
+        load.wait()
     for step in range(1, 2 * LINE):
         share_in(step).wait_recv()
     for block in sequence:
@@ -377,7 +509,20 @@
     closing = sum_ref[e, :, late_mine].astype(jnp.float32) + last_ref[...].astype(jnp.float32)
     out_ref[:, early:quarter] = closing.astype(jnp.bfloat16)
 
+    mixed_pair.wait_recv()
+    total = mixed_ref[mixed_rows(y), :].astype(jnp.float32)
+    mixer_ref[...] = (total + mixed_pair_ref[...].astype(jnp.float32)).astype(jnp.bfloat16)
+
     last.wait_send()
+    mixed_pair.wait_send()
+    for half in range(2):
+        mixed_core(half).wait_send()
+
+    @pl.when(e < 2 * LINE - 1)
+    def _():
+        halo_copy(0).wait_send()
+        halo_copy(1).wait_send()
+
     for part in (0, 1):
         @pl.when(z < LINE - 1)
         def _():
@@ -424,7 +569,9 @@
     lax.fori_loop(0, LINE, drained, 0)
 
 
-def expert_call(normed, share_of, gate_one, up_one, down_one):
+def layer_call(
+    normed, share_of, gate_one, up_one, down_one, queries, keys, values, sinks, project
+):
     tokens, width = normed.shape
     quarter = width // 4
     early = quarter * 5 // 8
@@ -432,12 +579,35 @@
     blocks = 2 * LINE
     kept = jnp.bfloat16
     dma = pltpu.SemaphoreType.DMA
+    span = queries.shape[0] // 4
+    in_vmem = pl.BlockSpec(memory_space=pltpu.VMEM)
+    in_smem = pl.BlockSpec(memory_space=pltpu.SMEM)
+    stays = pl.BlockSpec(memory_space=pl.ANY)
     return pl.pallas_call(
-        expert_kernel,
-        out_shape=jax.ShapeDtypeStruct((tokens, quarter), jnp.bfloat16),
-        in_specs=[pl.BlockSpec(memory_space=pltpu.VMEM)] * 5,
-        out_specs=pl.BlockSpec(memory_space=pltpu.VMEM),
+        layer_kernel,
+        out_shape=(
+            jax.ShapeDtypeStruct((span, width), kept),
+            jax.ShapeDtypeStruct((tokens, quarter), kept),
+        ),
+        in_specs=[in_vmem] * 2 + [stays] * 3 + [in_vmem] * 3 + [in_smem, stays],
+        out_specs=(in_vmem, in_vmem),
         scratch_shapes=[
+            pltpu.VMEM(gate_one.shape, kept),
+            pltpu.VMEM(up_one.shape, kept),
+            pltpu.VMEM(down_one.shape, kept),
+            pltpu.VMEM(project.shape, kept),
+            pltpu.VMEM((2, WINDOW_KEYS, keys.shape[1]), kept),
+            pltpu.VMEM(queries.shape, kept),
+            pltpu.VMEM((queries.shape[0], width), kept),
+            pltpu.VMEM((2, span, width), kept),
+            pltpu.VMEM((span, width), kept),
+            dma((4,)),
+            dma((2,)),
+            dma((2,)),
+            dma((2,)),
+            dma((2,)),
+            dma,
+            dma,
             pltpu.VMEM((blocks, tokens, width), kept),
             pltpu.VMEM((blocks, 8, tokens), jnp.float32),
             pltpu.VMEM((blocks, tokens, width), kept),
@@ -472,11 +642,11 @@
             collective_id=0, has_side_effects=True, vmem_limit_bytes=60 * 1024 * 1024
         ),
         cost_estimate=pl.CostEstimate(
-            flops=6 * blocks * tokens * width * gate_one.shape[1],
+            flops=8 * blocks * tokens * width * gate_one.shape[1],
             bytes_accessed=8 * width * gate_one.shape[1],
             transcendentals=0,
         ),
-    )(normed, share_of, gate_one, up_one, down_one)
+    )(normed, share_of, gate_one, up_one, down_one, queries, keys, values, sinks, project)
 
 
 def shards(
@@ -493,6 +663,32 @@
     up_weight,
     down_weight,
 ):
+    token_rows = expert_input.shape[0]
+    experts = lax.axis_size("ep")
+    capacity = max(3 * token_rows * TOPK // (2 * experts), 2)
+    col_share = D // lax.axis_size("tp")
+    widened = expert_input.astype(jnp.float32)
+    normed = (
+        widened
+        * lax.rsqrt(jnp.mean(widened * widened, axis=-1, keepdims=True) + EPS)
+        * norm_gain[None, :]
+    ).astype(jnp.bfloat16)
+    if (experts, lax.axis_size("tp")) == (2 * LINE, 4) and token_rows == 128:
+        named = routing == lax.broadcasted_iota(jnp.int32, (experts, 1, 1), 0)
+        share_of = jnp.sum(jnp.where(named, route_weight[None], 0.0), axis=2)
+        share_of = jnp.broadcast_to(share_of[:, None, :], (experts, 8, token_rows))
+        return layer_call(
+            normed,
+            share_of,
+            gate_weight[0],
+            up_weight[0],
+            down_weight[0],
+            projected_queries,
+            key_proj,
+            projected_values,
+            head_sink_logits,
+            out_weight,
+        )
     query_rows = projected_queries.shape[0]
     kv_heads = key_proj.shape[1] // HEAD_SIZE
     heads_per_group = projected_queries.shape[1] // HEAD_SIZE // kv_heads
@@ -547,59 +743,41 @@
         scatter_dimension=0,
         tiled=True,
     )
-    token_rows = expert_input.shape[0]
-    experts = lax.axis_size("ep")
-    capacity = max(3 * token_rows * TOPK // (2 * experts), 2)
-    col_share = D // lax.axis_size("tp")
-    widened = expert_input.astype(jnp.float32)
-    normed = (
-        widened
-        * lax.rsqrt(jnp.mean(widened * widened, axis=-1, keepdims=True) + EPS)
-        * norm_gain[None, :]
+    flat_ids = routing.reshape(-1)
+    onehot = (flat_ids[:, None] == jnp.arange(experts, dtype=jnp.int32)[None, :]).astype(jnp.int32)
+    rank_in = jnp.cumsum(onehot, axis=0) - 1
+    target = flat_ids * capacity + jnp.sum(rank_in * onehot, axis=1)
+    tok_ids = jnp.arange(token_rows * TOPK) // TOPK
+    slot_tok = jnp.full((experts * capacity,), token_rows, jnp.int32).at[target].set(tok_ids)
+    gate_one = gate_weight[0]
+    up_one = up_weight[0]
+    own_cols = lax.dynamic_slice_in_dim(normed, lax.axis_index("tp") * col_share, col_share, 1)
+    extended = jnp.concatenate([own_cols, jnp.zeros((1, col_share), jnp.bfloat16)], axis=0)
+    outgoing = jnp.take(extended, slot_tok, axis=0).reshape(experts, capacity, col_share)
+    arrived = lax.all_to_all(outgoing, "ep", split_axis=0, concat_axis=0, tiled=True).reshape(
+        experts * capacity, col_share
+    )
+    portion = lax.all_gather(arrived, "tp", axis=1, tiled=True)
+    gate_pre = jnp.dot(portion, gate_one, preferred_element_type=jnp.float32)
+    up_pre = jnp.dot(portion, up_one, preferred_element_type=jnp.float32)
+    gate_cut = jnp.minimum(gate_pre, CLAMP)
+    activated = (
+        (jnp.clip(up_pre, -CLAMP, CLAMP) + 1.0) * gate_cut * jax.nn.sigmoid(SLOPE * gate_cut)
     ).astype(jnp.bfloat16)
-    if (experts, lax.axis_size("tp")) != (2 * LINE, 4) or token_rows % 16:
-        flat_ids = routing.reshape(-1)
-        onehot = (flat_ids[:, None] == jnp.arange(experts, dtype=jnp.int32)[None, :]).astype(jnp.int32)
-        rank_in = jnp.cumsum(onehot, axis=0) - 1
-        target = flat_ids * capacity + jnp.sum(rank_in * onehot, axis=1)
-        tok_ids = jnp.arange(token_rows * TOPK) // TOPK
-        slot_tok = jnp.full((experts * capacity,), token_rows, jnp.int32).at[target].set(tok_ids)
-        gate_one = gate_weight[0]
-        up_one = up_weight[0]
-        own_cols = lax.dynamic_slice_in_dim(normed, lax.axis_index("tp") * col_share, col_share, 1)
-        extended = jnp.concatenate([own_cols, jnp.zeros((1, col_share), jnp.bfloat16)], axis=0)
-        outgoing = jnp.take(extended, slot_tok, axis=0).reshape(experts, capacity, col_share)
-        arrived = lax.all_to_all(outgoing, "ep", split_axis=0, concat_axis=0, tiled=True).reshape(
-            experts * capacity, col_share
-        )
-        portion = lax.all_gather(arrived, "tp", axis=1, tiled=True)
-        gate_pre = jnp.dot(portion, gate_one, preferred_element_type=jnp.float32)
-        up_pre = jnp.dot(portion, up_one, preferred_element_type=jnp.float32)
-        gate_cut = jnp.minimum(gate_pre, CLAMP)
-        activated = (
-            (jnp.clip(up_pre, -CLAMP, CLAMP) + 1.0) * gate_cut * jax.nn.sigmoid(SLOPE * gate_cut)
-        ).astype(jnp.bfloat16)
-        partial_value = jnp.dot(activated, down_weight[0], preferred_element_type=jnp.float32)
-        expert_result = lax.psum_scatter(
-            partial_value.astype(jnp.bfloat16), "tp", scatter_dimension=1, tiled=True
-        )
-        returned = lax.all_to_all(
-            expert_result.reshape(experts, capacity, col_share),
-            "ep",
-            split_axis=0,
-            concat_axis=0,
-            tiled=True,
-        )
-        picked = jnp.take(returned.reshape(experts * capacity, col_share), target, axis=0)
-        picked = picked.astype(jnp.float32).reshape(token_rows, TOPK, col_share)
-        expert_output = jnp.sum(picked * route_weight[:, :, None], axis=1).astype(jnp.bfloat16)
-    else:
-        named = routing == lax.broadcasted_iota(jnp.int32, (experts, 1, 1), 0)
-        share_of = jnp.sum(jnp.where(named, route_weight[None], 0.0), axis=2)
-        share_of = jnp.broadcast_to(share_of[:, None, :], (experts, 8, token_rows))
-        expert_output = expert_call(
-            normed, share_of, gate_weight[0], up_weight[0], down_weight[0]
-        )
+    partial_value = jnp.dot(activated, down_weight[0], preferred_element_type=jnp.float32)
+    expert_result = lax.psum_scatter(
+        partial_value.astype(jnp.bfloat16), "tp", scatter_dimension=1, tiled=True
+    )
+    returned = lax.all_to_all(
+        expert_result.reshape(experts, capacity, col_share),
+        "ep",
+        split_axis=0,
+        concat_axis=0,
+        tiled=True,
+    )
+    picked = jnp.take(returned.reshape(experts * capacity, col_share), target, axis=0)
+    picked = picked.astype(jnp.float32).reshape(token_rows, TOPK, col_share)
+    expert_output = jnp.sum(picked * route_weight[:, :, None], axis=1).astype(jnp.bfloat16)
     return (mixer_output, expert_output)
 
 

time: 155 us -> 120 us (0.77)
  between operations: 14.2 us -> 0.64 us
  starting transfers between devices: 8.34 us -> 0 us
  local copies, waits for them, and re-layouts: 11.2 us -> 4.16 us
  matrix products: 3.68 us -> 0 us
  Pallas kernels: 113 us -> 110 us
    ppermute x2 -> x0, starting transfers between devices: 8.3 us -> none  [passed_along(): return lax.ppermute(block, axis, route)]
    reshape x9 -> x0, local copies, waits for them, and re-layouts: 3.74 us -> none  [the longest x1 1.26 us: shards(): projected_queries.reshape(count_of_blocks, WINDOW_KEYS, kv_heads, heads_p...]
    dot_general x3 -> x0, matrix products: 3.68 us -> none  [the longest x1 2.67 us: shards(): jnp.dot(attended, out_weight, preferred_element_type=jnp.float32)]
    pallas_call x1, Pallas kernels: 113 us -> 110 us  [layer_call(): pl.pallas_call(layer_kernel, out_shape=(jax.ShapeDtypeStruct((span, width...]
    unnamed x13 -> x2, local copies, waits for them, and re-layouts: 4.32 us -> 3.54 us
  transfers between devices with their start and end apart: 3 -> 0, of which waited for: 0 -> 0; matrix products, arithmetic and copies ran while one was open for 6% -> 0% of each run, Pallas kernels for 74% -> 0%
where the time goes in v2:
time: 120 us
  Pallas kernels  110 us (92%)
  other arithmetic  4.78 us (4%)
  local copies, waits for them, and re-layouts  4.16 us (3%)
    pallas_call x1, Pallas kernels, layer_call(): pl.pallas_call(layer_kernel, out_shape=(jax.ShapeDtypeStruct((span, width...  110 us
    unnamed x2, local copies, waits for them, and re-layouts  3.54 us
    convert_element_type x1, other arithmetic, shards(): normed = (widened * lax.rsqrt(jnp.mean(widened * widened, axis=-1, keepdi...  2.54 us

profile of v2, /device:TPU:0, one launch (start us, length us, event | category | flops | bytes accessed | tf_op | source)
XLA Modules:
  0.0 119.8 jit_solution(9339744168941346666)
XLA Ops:
  0.6 1.5 %fusion = f32[128]{0:T(128)S(1)} fusion(bf16[128,4096]{1,0:T(8,128)(2,1)} %param.17), kind=kLoop, calls=%fused_computation.2 | loop fusion | flops 1572736 | bytes 1049088 | tf_op jit(solution)/shard_map/reduce_sum | solution.py:673
  2.2 0.7 select_reduce_fusion
  2.9 0.6 broadcast_in_dim.24.share_ref
  3.5 2.5 %fusion.2.own_ref = bf16[128,4096]{1,0:T(8,128)(2,1)} fusion(bf16[128,4096]{1,0:T(8,128)(2,1)} %param.17, f32[4096]{0:T(1024)} %param.18, f32[128]{0:T(128)S(1)} %add_rsqrt_fusion), kind=kLoop, calls=%fused_computation.4 | loop fusion | flops 2097152 | bytes 2114048 | tf_op jit(solution)/shard_map/convert_element_type | solution.py:675
  6.0 110.3 %shard_map.131 = (bf16[64,4096]{1,0:T(8,128)(2,1)}, bf16[128,1024]{1,0:T(8,128)(2,1)}) custom-call(bf16[128,4096]{1,0:T(8,128)(2,1)} %fusion.2.own_ref, f32[8,8,128]{2,1,0:T(8,128)} %broadcast_in_dim.24.share_ref, bf16[4096,256]{1,0:T(8,128)(2,1)} %bitcast.3, bf16[4096,256]{1,0:T(8,128)(2,1)} %bitcast.4, bf16[256,4096]{1,0:T(8,128)(2,1)} %bitcast.5, ...), custom_call_target="tpu_custom_call" | custom-call | flops 8589934592 | bytes 8388608 | tf_op jit(solution)/shard_map/pallas_call | solution.py:586
  116.3 1.9 %copy.18 = bf16[64,4096]{1,0:T(8,128)(2,1)} copy(bf16[64,4096]{1,0:T(8,128)(2,1)} %get-tuple-element.4) | data formatting | bytes 1048576
  118.2 1.7 %copy.19 = bf16[128,1024]{1,0:T(8,128)(2,1)} copy(bf16[128,1024]{1,0:T(8,128)(2,1)} %get-tuple-element.5) | data formatting | bytes 524288
  (1 shorter events, 0.0 us)

commit v3 on v2

--- a/solution.py
+++ b/solution.py
@@ -38,7 +38,8 @@
 
 
 def layer_kernel(
-    own_ref,
+    token_ref,
+    gain_ref,
     share_ref,
     gate_hbm,
     up_hbm,
@@ -50,6 +51,7 @@
     project_hbm,
     mixer_ref,
     out_ref,
+    own_ref,
     gate_ref,
     up_ref,
     down_ref,
@@ -98,8 +100,7 @@
 ):
     e, t = lax.axis_index("ep"), lax.axis_index("tp")
     z, x, y, c = e // 2, e % 2, t // 2, t % 2
-    width = own_ref.shape[1]
-    tokens = own_ref.shape[0]
+    tokens, width = token_ref.shape
     sibling, partner, beside = (e, y * 2 + 1 - c), (e, (1 - y) * 2 + c), (z * 2 + 1 - x, t)
     above, below = (e + 2, t), (e - 2, t)
 
@@ -123,6 +124,10 @@
         )
     for other in (sibling, partner):
         pl.semaphore_signal(barrier, inc=1, device_id=other, device_id_type=MESH)
+    widened = token_ref[...].astype(jnp.float32)
+    scale = lax.rsqrt(jnp.mean(widened * widened, axis=-1, keepdims=True) + EPS)
+    own_ref[...] = (widened * scale * gain_ref[...]).astype(jnp.bfloat16)
+    rows_ref[e] = own_ref[...]
     pl.semaphore_wait(barrier, 2 * LINE + 1)
 
     lone = width * 3 // 16
@@ -217,7 +222,6 @@
 
     for step in range(1, 2 * LINE):
         share_copy(step).start()
-    rows_ref[e] = own_ref[...]
     weight_ref[e] = share_ref[e]
 
     kv_heads = key_ref.shape[1] // HEAD_SIZE
@@ -300,7 +304,6 @@
             mixed_ref[mixed_rows(half), :] = (
                 total + mixed_core_ref[half].astype(jnp.float32)
             ).astype(jnp.bfloat16)
-        mixed_pair.start()
 
     mix()
     near = [chosen(z, [nearest_first(place)[j] for place in range(LINE)]) for j in range(LINE)]
@@ -457,6 +460,10 @@
 
             lax.fori_loop(0, 2, one, 0)
 
+        @pl.when(i == LINE)
+        def _():
+            mixed_pair.start()
+
         @pl.when((i >= 2) & (i < LINE + 2))
         def _():
             at = far(i - 2)
@@ -570,9 +577,9 @@
 
 
 def layer_call(
-    normed, share_of, gate_one, up_one, down_one, queries, keys, values, sinks, project
+    rows, gain, share_of, gate_one, up_one, down_one, queries, keys, values, sinks, project
 ):
-    tokens, width = normed.shape
+    tokens, width = rows.shape
     quarter = width // 4
     early = quarter * 5 // 8
     carried = quarter + quarter - early
@@ -589,9 +596,10 @@
             jax.ShapeDtypeStruct((span, width), kept),
             jax.ShapeDtypeStruct((tokens, quarter), kept),
         ),
-        in_specs=[in_vmem] * 2 + [stays] * 3 + [in_vmem] * 3 + [in_smem, stays],
+        in_specs=[in_vmem] * 3 + [stays] * 3 + [in_vmem] * 3 + [in_smem, stays],
         out_specs=(in_vmem, in_vmem),
         scratch_shapes=[
+            pltpu.VMEM(rows.shape, kept),
             pltpu.VMEM(gate_one.shape, kept),
             pltpu.VMEM(up_one.shape, kept),
             pltpu.VMEM(down_one.shape, kept),
@@ -646,7 +654,7 @@
             bytes_accessed=8 * width * gate_one.shape[1],
             transcendentals=0,
         ),
-    )(normed, share_of, gate_one, up_one, down_one, queries, keys, values, sinks, project)
+    )(rows, gain, share_of, gate_one, up_one, down_one, queries, keys, values, sinks, project)
 
 
 def shards(
@@ -678,7 +686,8 @@
         share_of = jnp.sum(jnp.where(named, route_weight[None], 0.0), axis=2)
         share_of = jnp.broadcast_to(share_of[:, None, :], (experts, 8, token_rows))
         return layer_call(
-            normed,
+            expert_input,
+            norm_gain[None, :],
             share_of,
             gate_weight[0],
             up_weight[0],

time: 120 us -> 114 us (0.950)
  other arithmetic: 4.78 us -> 0.71 us
  Pallas kernels: 110 us -> 108 us
    convert_element_type x1 -> x0, other arithmetic: 2.54 us -> none  [shards(): normed = (widened * lax.rsqrt(jnp.mean(widened * widened, axis=-1, keepdi...]
    pallas_call x1, Pallas kernels: 110 us -> 108 us  [layer_call(): pl.pallas_call(layer_kernel, out_shape=(jax.ShapeDtypeStruct((span, width...]
    reduce_sum x1 -> x0, other arithmetic: 1.52 us -> none  [shards(): jnp.mean(widened * widened, axis=-1, keepdims=True) + EPS]
where the time goes in v3:
time: 114 us
  Pallas kernels  108 us (95%)
  local copies, waits for them, and re-layouts  4.16 us (4%)
    pallas_call x1, Pallas kernels, layer_call(): pl.pallas_call(layer_kernel, out_shape=(jax.ShapeDtypeStruct((span, width...  108 us
    unnamed x2, local copies, waits for them, and re-layouts  3.54 us

profile of v3, /device:TPU:0, one launch (start us, length us, event | category | flops | bytes accessed | tf_op | source)
XLA Modules:
  0.0 114.0 jit_solution(18118232150314239206)
XLA Ops:
  0.6 0.7 select_reduce_fusion
  1.3 0.6 broadcast_in_dim.26.share_ref
  2.0 108.5 %shard_map.131 = (bf16[64,4096]{1,0:T(8,128)(2,1)}, bf16[128,1024]{1,0:T(8,128)(2,1)}) custom-call(bf16[128,4096]{1,0:T(8,128)(2,1)} %token_ref.1, f32[1,4096]{1,0:T(1,128)} %bitcast.7, f32[8,8,128]{2,1,0:T(8,128)} %broadcast_in_dim.26.share_ref, bf16[4096,256]{1,0:T(8,128)(2,1)} %bitcast.4, bf16[4096,256]{1,0:T(8,128)(2,1)} %bitcast.5, ...), custom_call_target="tpu_custom_call" | custom-call | flops 8589934592 | bytes 8388608 | tf_op jit(solution)/shard_map/pallas_call | solution.py:593
  110.4 1.9 %copy.18 = bf16[64,4096]{1,0:T(8,128)(2,1)} copy(bf16[64,4096]{1,0:T(8,128)(2,1)} %get-tuple-element.4) | data formatting | bytes 1048576
  112.3 1.7 %copy.19 = bf16[128,1024]{1,0:T(8,128)(2,1)} copy(bf16[128,1024]{1,0:T(8,128)(2,1)} %get-tuple-element.5) | data formatting | bytes 524288
